TPU v7x, 32 devices: a whole 2x2x4 slice. The times are simulated.
32 devices in a mesh: fs: 8 (over z, x), tp: 4 (over y, core).
Axes of the slice: x: 2, y: 2, z: 4, core: 2. Of those that a mesh axis runs over, the one named last changes fastest.
Arguments:
- h_saved: bfloat16 [16384, 2048], P('fs'), may hold values from -6 to 6
- conv_cotan: bfloat16 [16384, 2560], P('fs', 'tp'), may hold values from -64 to 64
- lru_out: bfloat16 [16384, 2560], P('fs', 'tp'), may hold values from -64 to 64
- out_cotan: bfloat16 [16384, 2048], P('fs'), may hold values from -6 to 6
- basis_in: bfloat16 [2048, 256], P('fs'), may hold values from -1.41421356 to 1.41421356
- basis_out: bfloat16 [2048, 256], P('fs'), may hold values from -1.41421356 to 1.41421356
- weight_in: float32 [2048, 2560], P('fs', 'tp'), may hold values from -0.125 to 0.125
- weight_out: float32 [2560, 2048], P('tp', 'fs'), may hold values from -0.125 to 0.125
- first_in: float32 [256, 2560], P('fs', 'tp'), may hold values from -6 to 6
- second_in: float32 [256, 2560], P('fs', 'tp'), may hold values from 0.05 to 2
- first_out: float32 [256, 2560], P('fs', 'tp'), may hold values from -6 to 6
- second_out: float32 [256, 2560], P('fs', 'tp'), may hold values from 0.05 to 2
Outputs:
- step_in: float32 [2048, 2560], P('fs', 'tp')
- new_weight_in: float32 [2048, 2560], P('fs', 'tp')
- copy_in: bfloat16 [2048, 2560], P(None, 'tp')
- new_first_in: float32 [256, 2560], P('fs', 'tp')
- new_second_in: float32 [256, 2560], P('fs', 'tp')
- step_out: float32 [2560, 2048], P('tp', 'fs')
- new_weight_out: float32 [2560, 2048], P('tp', 'fs')
- copy_out: bfloat16 [2560, 2048], P('tp')
- new_first_out: float32 [256, 2560], P('fs', 'tp')
- new_second_out: float32 [256, 2560], P('fs', 'tp')
All inputs are finite; a program needn't handle non-finite values.
Results may differ from a plain program's by a relative error of at most 0.0046.
Values may be sent and summed in bfloat16 or wider, within the bound.
A program may use at most 128 MiB of HBM per device.

v0:
```python
import functools
import math

import jax
import jax.numpy as jnp
from jax import lax
from jax.experimental import pallas as pl
from jax.experimental.pallas import tpu as pltpu
from jax.sharding import PartitionSpec as P

MESH = pl.DeviceIdType.MESH
VMEM_LIMIT = 60 * 1024 * 1024


def nt_dot(left, right):
    return lax.dot_general(left, right, (((1,), (1,)), ((), ())), preferred_element_type=jnp.float32)


def exchange(
    dims,
    h_hbm,
    cc_hbm,
    oc_hbm,
    lo_hbm,
    basis_in,
    basis_out,
    w_in,
    w_out,
    m_in,
    v_in,
    m_out,
    v_out,
    ball,
    win_all,
    wout_all,
    dall,
    nm_in,
    nv_in,
    nm_out,
    nv_out,
    h_buf,
    c_buf,
    acc,
    part,
    part_in,
    tot,
    tot_two,
    tot_in,
    in_sem,
    ss,
    rs,
    cs,
    cr,
    ps,
    pr,
    ts,
    tr,
):
    F, T, Z, X, scale = dims
    f = lax.axis_index("fs")
    t = lax.axis_index("tp")
    z, x = f // X, f % X
    core = t % 2
    mate = t + 1 - 2 * core
    tokens, chunk = h_buf.shape[1], h_buf.shape[1] // in_sem.shape[1]
    chunks = in_sem.shape[1]
    rr = m_in.shape[0]

    def fetch(which, i):
        rows = pl.ds(i * chunk, chunk)
        h_src, c_src = ((h_hbm, cc_hbm), (oc_hbm, lo_hbm))[which]
        return (
            pltpu.make_async_copy(h_src.at[rows], h_buf.at[which, rows], in_sem.at[which, i, 0]),
            pltpu.make_async_copy(c_src.at[rows], c_buf.at[which, rows], in_sem.at[which, i, 1]),
        )

    for which in range(2):
        for i in range(chunks):
            for copy in fetch(which, i):
                copy.start()

    barrier = pltpu.get_barrier_semaphore()

    def greet(n, carry):
        pl.semaphore_signal(
            barrier, inc=1, device_id=((f + n // T) % F, (t + n % T) % T), device_id_type=MESH
        )
        return carry

    lax.fori_loop(1, F * T, greet, 0)
    for which, basis in enumerate((basis_in, basis_out)):
        ball[which, f] = basis[...]
    win_all[f] = w_in[...].astype(jnp.bfloat16)
    wout_all[f] = w_out[...].astype(jnp.bfloat16)
    pl.semaphore_wait(barrier, F * T - 1)

    def source(k, j):
        return ((z + Z - k) % Z) * X + (x + X - j) % X

    half = basis_in.shape[0] // 2
    q_in, q_out = w_in.shape[0] // 2, w_out.shape[0] // 2

    def place(item, s, core):
        if item < 2:
            return ball.at[item, s, pl.ds(pl.multiple_of(core * half, half), half)]
        if item < 4:
            return win_all.at[s, pl.ds((item - 2) * q_in, q_in)]
        if item < 6:
            return wout_all.at[s, pl.ds((item - 4) * q_out, q_out)]
        return dall.at[item - 6, s]

    def own(item):
        if item < 2:
            return (basis_in, basis_out)[item].at[pl.ds(pl.multiple_of(core * half, half), half)]
        return place(item, f, core)

    def along_z(item, k, src=None):
        at = place(item, f, core)
        return pltpu.make_async_remote_copy(
            src_ref=at if src is None else src,
            dst_ref=at,
            send_sem=ss.at[item, k, 0],
            recv_sem=rs.at[item, k, 0],
            device_id=(((z + k) % Z) * X + x, t),
            device_id_type=MESH,
        )

    def along_x(item, k, j, src=None):
        at = place(item, source(k, 0), core)
        return pltpu.make_async_remote_copy(
            src_ref=at if src is None else src,
            dst_ref=at,
            send_sem=ss.at[item, k, j],
            recv_sem=rs.at[item, k, j],
            device_id=(z * X + (x + j) % X, t),
            device_id_type=MESH,
        )

    def across(item, k, j, side=None):
        at = place(item, source(k, j), core if side is None else side)
        return pltpu.make_async_remote_copy(
            src_ref=at,
            dst_ref=at,
            send_sem=cs.at[item, k, j],
            recv_sem=cr.at[item, k, j],
            device_id=(f, mate),
            device_id_type=MESH,
        )

    def arrived(item, k, j):
        at = place(item, source(k, j), core)
        pltpu.make_async_remote_copy(
            src_ref=at,
            dst_ref=at,
            send_sem=ss.at[item, k, j],
            recv_sem=rs.at[item, k, j],
            device_id=((f + 1) % F, t),
            device_id_type=MESH,
        ).wait_recv()

    def begin(item):
        src = own(item)
        for k in range(1, Z):
            along_z(item, k, src).start()
        for j in range(1, X):
            along_x(item, 0, j, src).start()

    def forward(item):
        for k in range(1, Z):
            arrived(item, k, 0)
            for j in range(1, X):
                along_x(item, k, j).start()
            if item < 2:
                across(item, k, 0).start()

    def finish(item):
        for k in range(Z):
            for j in range(1, X):
                arrived(item, k, j)
                if item < 2:
                    across(item, k, j).start()
        if item < 2:
            for k in range(Z):
                for j in range(X):
                    if k or j:
                        across(item, k, j, 1 - core).wait_recv()

    def drain(item):
        for k in range(Z):
            for j in range(X):
                if j:
                    along_x(item, k, j).wait_send()
                elif k:
                    along_z(item, k).wait_send()
                if item < 2 and (k or j):
                    across(item, k, j).wait_send()

    def project(which):
        acc[which] = jnp.zeros(acc.shape[1:], jnp.float32)

        def step(i, carry):
            for copy in fetch(which, i):
                copy.wait()
            rows = pl.ds(pl.multiple_of(i * chunk, chunk), chunk)
            whole = ball[which].reshape(h_buf.shape[2], -1)
            reduced = jnp.dot(h_buf[which, rows], whole, preferred_element_type=jnp.float32)
            turned = reduced.T
            upper = turned.astype(jnp.bfloat16)
            lower = (turned - upper.astype(jnp.float32)).astype(jnp.bfloat16)
            block = c_buf[which, rows]
            acc[which] += jnp.dot(upper, block, preferred_element_type=jnp.float32) + jnp.dot(
                lower, block, preferred_element_type=jnp.float32
            )
            return carry

        lax.fori_loop(0, chunks, step, 0)
        part[which] = acc[which].astype(jnp.bfloat16).reshape(part.shape[1:])

    def scatter(which, d):
        peer = (f + d) % F
        return pltpu.make_async_remote_copy(
            src_ref=part.at[which, peer],
            dst_ref=part_in.at[which, d],
            send_sem=ps.at[which, d],
            recv_sem=pr.at[which, d],
            device_id=(peer, t),
            device_id_type=MESH,
        )

    def share(n):
        return pltpu.make_async_remote_copy(
            src_ref=tot,
            dst_ref=tot_in.at[n],
            send_sem=ts.at[n],
            recv_sem=tr.at[n],
            device_id=(f, (t + n) % T),
            device_id_type=MESH,
        )

    def share_on(d):
        return pltpu.make_async_remote_copy(
            src_ref=tot_two,
            dst_ref=tot_in.at[T + d],
            send_sem=ts.at[T + d],
            recv_sem=tr.at[T + d],
            device_id=((f + d) % F, t),
            device_id_type=MESH,
        )

    begin(0)
    begin(1)
    forward(0)
    forward(1)
    begin(2)
    finish(0)
    project(0)
    for d in range(1, F):
        scatter(0, d).start()
    finish(1)
    project(1)
    for d in range(1, F):
        scatter(1, d).start()
    forward(2)
    begin(3)
    projs = []
    square = jnp.zeros((1, 1), jnp.float32)
    for which in range(2):
        value = acc[which, pl.ds(pl.multiple_of(f * rr, rr), rr)]
        for d in range(1, F):
            scatter(which, d).wait_recv()
            value = value + part_in[which, d].astype(jnp.float32)
        projs.append(value)
        square = square + jnp.sum(value * value, axis=(0, 1), keepdims=True)
    tot[...] = jnp.broadcast_to(square, tot.shape)
    tot_in[0] = tot[...]

    for n in range(1, T):
        share(n).start()
    for n in range(1, T):
        share(n).wait()
    tot_two[...] = jnp.sum(tot_in[:T], axis=0)
    tot_in[T] = tot_two[...]
    for d in range(1, F):
        share_on(d).start()
    for d in range(1, F):
        share_on(d).wait()
    total = jnp.sum(tot_in[T:], axis=0)
    factor = (scale * lax.rsqrt(total + 1e-06))[0:1, 0:1]
    for which, (first, second, first_to, second_to) in enumerate(
        ((m_in, v_in, nm_in, nv_in), (m_out, v_out, nm_out, nv_out))
    ):
        scaled = factor * projs[which]
        first_new = 0.8 * first[...] + 0.2 * scaled
        second_new = 0.9 * second[...] + 0.1 * scaled * scaled
        first_to[...] = first_new
        second_to[...] = second_new
        dall[which, f] = (first_new / (jnp.sqrt(second_new) + 1e-08)).astype(jnp.bfloat16)
    begin(6)
    begin(7)
    begin(4)
    begin(5)
    forward(3)
    forward(6)
    forward(7)
    forward(4)
    forward(5)
    for item in (2, 3, 6, 7, 4, 5):
        finish(item)
    for item in range(8):
        drain(item)
    for which in range(2):
        for d in range(1, F):
            scatter(which, d).wait_send()


def apply_step(
    basis_in, basis_out, w_in, w_out, nm_in, nv_in, nm_out, nv_out, b_in, b_out, win, wout, dirs,
    step_in, new_in, copy_in, o_m_in, o_v_in, step_out, new_out, copy_out, o_m_out, o_v_out, turned,
):
    direction = dirs[0].reshape(-1, dirs.shape[3])

    @pl.when(pl.program_id(0) == 0)
    def _():
        other = dirs[1].reshape(-1, dirs.shape[3])
        turned[...] = other.astype(jnp.float32).T.astype(jnp.bfloat16)
        for source, target in ((nm_in, o_m_in), (nv_in, o_v_in), (nm_out, o_m_out), (nv_out, o_v_out)):
            target[...] = source[...]
        step = jnp.dot(basis_in[...], direction, preferred_element_type=jnp.float32)
        step_in[...] = step
        new_in[...] = w_in[...] - 0.02 * step
        step = nt_dot(turned[...], basis_out[...])
        step_out[...] = step
        new_out[...] = w_out[...] - 0.02 * step

    step = jnp.dot(b_in[0, 0], direction, preferred_element_type=jnp.float32)
    copy_in[...] = (win[0].astype(jnp.float32) - 0.02 * step).astype(jnp.bfloat16)
    step = nt_dot(turned[...], b_out[0, 0])
    copy_out[...] = (wout[0].astype(jnp.float32) - 0.02 * step).astype(jnp.bfloat16)


def shards(mesh, h, cc, lo, oc, basis_in, basis_out, w_in, w_out, m_in, v_in, m_out, v_out):
    F, T = mesh.shape["fs"], mesh.shape["tp"]
    Z = next(n for n in range(1, F + 1) if F % n == 0 and n * n >= F)
    X = F // Z
    tokens, model = h.shape
    cols = cc.shape[1]
    rows, rank = basis_in.shape
    rr = m_in.shape[0]
    scale = math.sqrt(2.0 * rank * cols * T)
    chunks = max(1, tokens // 512)
    bf, f32 = jnp.bfloat16, jnp.float32
    hbm = pl.BlockSpec(memory_space=pl.ANY)
    vmem = pl.BlockSpec(memory_space=pltpu.VMEM)
    moment = jax.ShapeDtypeStruct(m_in.shape, f32)
    dma = pltpu.SemaphoreType.DMA
    ball, win_all, wout_all, dall, *moments = pl.pallas_call(
        functools.partial(exchange, (F, T, Z, X, scale)),
        out_shape=(
            jax.ShapeDtypeStruct((2, F, rows, rank), bf),
            jax.ShapeDtypeStruct((F,) + w_in.shape, bf),
            jax.ShapeDtypeStruct((F,) + w_out.shape, bf),
            jax.ShapeDtypeStruct((2, F, rr, cols), bf),
            moment,
            moment,
            moment,
            moment,
        ),
        in_specs=[hbm] * 4 + [vmem] * 8,
        out_specs=(vmem,) * 8,
        scratch_shapes=[
            pltpu.VMEM((2, tokens, model), bf),
            pltpu.VMEM((2, tokens, cols), bf),
            pltpu.VMEM((2, rank, cols), f32),
            pltpu.VMEM((2, F, rr, cols), bf),
            pltpu.VMEM((2, F, rr, cols), bf),
            pltpu.VMEM((8, 128), f32),
            pltpu.VMEM((8, 128), f32),
            pltpu.VMEM((T + F, 8, 128), f32),
            dma((2, chunks, 2)),
            dma((8, Z, X)),
            dma((8, Z, X)),
            dma((2, Z, X)),
            dma((2, Z, X)),
            dma((2, F)),
            dma((2, F)),
            dma((T + F,)),
            dma((T + F,)),
        ],
        compiler_params=pltpu.CompilerParams(
            collective_id=0, has_side_effects=True, vmem_limit_bytes=VMEM_LIMIT
        ),
        name="exchange",
    )(h, cc, oc, lo, basis_in, basis_out, w_in, w_out, m_in, v_in, m_out, v_out)

    def fixed(array):
        return pl.BlockSpec(array.shape, lambda i, n=array.ndim: (0,) * n)

    keep = (basis_in, basis_out, w_in, w_out, *moments)
    outs = (
        (w_in.shape, f32, None),
        (w_in.shape, f32, None),
        ((model, cols), bf, pl.BlockSpec(w_in.shape, lambda i: (i, 0))),
        (m_in.shape, f32, None),
        (m_in.shape, f32, None),
        (w_out.shape, f32, None),
        (w_out.shape, f32, None),
        ((cols, model), bf, pl.BlockSpec(w_out.shape, lambda i: (0, i))),
        (m_in.shape, f32, None),
        (m_in.shape, f32, None),
    )
    return pl.pallas_call(
        apply_step,
        grid=(F,),
        out_shape=tuple(jax.ShapeDtypeStruct(shape, kind) for shape, kind, _ in outs),
        in_specs=[fixed(a) for a in keep]
        + [
            pl.BlockSpec((1, 1, rows, rank), lambda i: (0, i, 0, 0)),
            pl.BlockSpec((1, 1, rows, rank), lambda i: (1, i, 0, 0)),
            pl.BlockSpec((1,) + w_in.shape, lambda i: (i, 0, 0)),
            pl.BlockSpec((1,) + w_out.shape, lambda i: (i, 0, 0)),
            fixed(dall),
        ],
        out_specs=tuple(
            spec or pl.BlockSpec(shape, lambda i, n=len(shape): (0,) * n) for shape, _, spec in outs
        ),
        scratch_shapes=[pltpu.VMEM((cols, rank), bf)],
        compiler_params=pltpu.CompilerParams(vmem_limit_bytes=VMEM_LIMIT),
        name="apply_step",
    )(*keep, ball, ball, win_all, wout_all, dall)


def solution(mesh):
    split, both = P("fs", None), P("fs", "tp")
    return jax.shard_map(
        functools.partial(shards, mesh),
        mesh=mesh,
        in_specs=(split, both, both, split, split, split, both, P("tp", "fs"), both, both, both, both),
        out_specs=(both, both, P(None, "tp"), both, both, P("tp", "fs"), P("tp", "fs"), P("tp", None), both, both),
        check_vma=False,
    )
```

profile of v0, /device:TPU:0, one launch (start us, length us, event | category | flops | bytes accessed | tf_op | source)
XLA Modules:
  0.0 129.6 jit_solution(12068118023572585624)
XLA Ops:
  0.6 118.1 %exchange.1 = (bf16[2,8,256,256]{3,2,1,0:T(8,128)(2,1)}, bf16[8,256,640]{2,1,0:T(8,128)(2,1)}, bf16[8,640,256]{2,1,0:T(8,128)(2,1)}, bf16[2,8,32,640]{3,2,1,0:T(...) custom-call(bf16[2048,2048]{1,0:T(8,128)(2,1)} %h_hbm.1, ...), custom_call_target="tpu_custom_call" | custom-call | tf_op jit(solution)/shard_map/exchange/pallas_call | solution.py:356
  118.7 10.8 %apply_step.1 = (f32[256,640]{1,0:T(8,128)}, f32[256,640]{1,0:T(8,128)}, bf16[2048,640]{1,0:T(8,128)(2,1)}, f32[32,640]{1,0:T(8,128)}, f32[32,640]{1,0:T(8,128)}...) custom-call(bf16[256,256]{1,0:T(8,128)(2,1)} %basis_in.3, ...), custom_call_target="tpu_custom_call" | custom-call | tf_op jit(solution)/shard_map/apply_step/pallas_call | solution.py:411
where the time goes:
time: 130 us
  Pallas kernels  129 us (99%)
    pallas_call x1, Pallas kernels, shards(): pl.pallas_call(functools.partial(exchange, (F, T, Z, X, scale)), out_shap...  118 us
    pallas_call x1, Pallas kernels, shards(): pl.pallas_call(apply_step, grid=(F,), out_shape=tuple((jax.ShapeDtypeStru...  10.8 us

commit v1 on v0

v1 whole, which is shorter than its diff:
```python
import functools
import math

import jax
import jax.numpy as jnp
from jax import lax
from jax.experimental import pallas as pl
from jax.experimental.pallas import tpu as pltpu
from jax.sharding import PartitionSpec as P

MESH = pl.DeviceIdType.MESH
VMEM_LIMIT = 42 * 1024 * 1024
FLUSH_LIMIT = 1024 * 1024
PIECES = 8
WINDOW = 3
AHEAD = 4


def nt_dot(left, right):
    return lax.dot_general(left, right, (((1,), (1,)), ((), ())), preferred_element_type=jnp.float32)


def exchange(
    dims,
    h_hbm,
    cc_hbm,
    oc_hbm,
    lo_hbm,
    basis_in,
    basis_out,
    w_in,
    w_out,
    m_in,
    v_in,
    m_out,
    v_out,
    step_in,
    new_in,
    copy_in,
    nm_in,
    nv_in,
    step_out,
    new_out,
    copy_out,
    nm_out,
    nv_out,
    ball,
    win_all,
    wout_all,
    dall,
    turned,
    h_buf,
    c_buf,
    acc,
    part,
    x_part,
    z_sum,
    z_part,
    tot,
    tot_in,
    in_sem,
    bx_s,
    bx_r,
    bz_s,
    bz_r,
    by_s,
    by_r,
    bm_s,
    bm_r,
    px_s,
    px_r,
    pz_s,
    pz_r,
    tot_s,
    tot_r,
    dx_s,
    dx_r,
    dz_s,
    dz_r,
    wd_s,
    wd_r,
    wu_s,
    wu_r,
    wx_s,
    wx_r,
):
    F, T, Z, X, scale = dims
    Y, Q = T // 2, PIECES
    f = lax.axis_index("fs")
    t = lax.axis_index("tp")
    z, x = f // X, f % X
    y, core = t // 2, t % 2
    mate = t + 1 - 2 * core
    turn = 1 - 2 * ((2 * z) // Z)
    chunks = in_sem.shape[1]
    chunk = h_buf.shape[1] // chunks
    rr, cols = m_in.shape
    rows, rank = basis_in.shape
    quarter = rows // T

    def remote(src, dst, send, recv, device):
        return pltpu.make_async_remote_copy(
            src_ref=src, dst_ref=dst, send_sem=send, recv_sem=recv, device_id=device, device_id_type=MESH
        )

    def z_peer(k):
        return ((z + k) % Z) * X + x

    def x_peer(j):
        return z * X + (x + j) % X

    def fetch(which, i):
        span = pl.ds(i * chunk, chunk)
        h_src, c_src = ((h_hbm, cc_hbm), (oc_hbm, lo_hbm))[which]
        return (
            pltpu.make_async_copy(h_src.at[span], h_buf.at[which, span], in_sem.at[which, i, 0]),
            pltpu.make_async_copy(c_src.at[span], c_buf.at[which, span], in_sem.at[which, i, 1]),
        )

    barrier = pltpu.get_barrier_semaphore()

    def greet(device):
        pl.semaphore_signal(barrier, inc=1, device_id=device, device_id_type=MESH)

    for k in range(1, Z):
        greet((z_peer(k), t))
    for j in range(1, X):
        greet((x_peer(j), t))
    for i in range(1, Y):
        greet((f, ((y + i) % Y) * 2 + core))
    greet((f, mate))
    for which in range(2):
        for i in range(chunks):
            for copy in fetch(which, i):
                copy.start()
    own = pl.ds(pl.multiple_of(t * quarter, quarter), quarter)
    for which, basis in enumerate((basis_in, basis_out)):
        ball[which, f] = basis[...]
    win_all[f] = w_in[...].astype(jnp.bfloat16)
    wout_all[f] = w_out[...].astype(jnp.bfloat16)
    pl.semaphore_wait(barrier, (Z - 1) + (X - 1) + (Y - 1) + 1)

    def row(m):
        return (z + turn * m + Z) % Z

    def basis_at(which, m, j, part_of):
        s = row(m) * X + (x + X - j) % X
        return ball.at[which, s, pl.ds(pl.multiple_of(part_of * quarter, quarter), quarter)]

    def basis_z(which, k):
        src = (basis_in, basis_out)[which].at[own]
        return remote(
            src, ball.at[which, f, own], bz_s.at[which, k], bz_r.at[which, z], (z_peer(k), t)
        )

    def basis_z_arrival(which, m):
        at = basis_at(which, m, 0, t)
        return remote(at, at, bz_s.at[which, m], bz_r.at[which, row(m)], (z_peer(1), t))

    def basis_x(which, m, j):
        at = basis_at(which, m, 0, t)
        src = at if m else (basis_in, basis_out)[which].at[own]
        return remote(src, at, bx_s.at[which, m, j], bx_r.at[which, m, j], (x_peer(j), t))

    def basis_x_arrival(which, m, j):
        at = basis_at(which, m, j, t)
        return remote(at, at, bx_s.at[which, m, j], bx_r.at[which, m, j], (x_peer(j), t))

    def basis_y(which, m, j, i, arrival=False):
        at = basis_at(which, m, j, ((y + Y - i) % Y) * 2 + core if arrival else t)
        return remote(
            at, at, by_s.at[which, m, j, i], by_r.at[which, m, j, i], (f, ((y + i) % Y) * 2 + core)
        )

    def basis_mate(which, m, j, i, arrival=False):
        at = basis_at(which, m, j, ((y + Y - i) % Y) * 2 + (1 - core if arrival else core))
        return remote(at, at, bm_s.at[which, m, j, i], bm_r.at[which, m, j, i], (f, mate))

    def basis_begin(which):
        for k in range(1, Z):
            basis_z(which, k).start()
        for j in range(1, X):
            basis_x(which, 0, j).start()

    def basis_spread(which, m, j):
        for i in range(1, Y):
            basis_y(which, m, j, i).start()
        basis_mate(which, m, j, 0).start()

    def basis_over_z(which):
        for m in range(1, Z):
            basis_z_arrival(which, m).wait_recv()
            for j in range(1, X):
                basis_x(which, m, j).start()
            basis_spread(which, m, 0)

    def basis_over_x(which):
        for m in range(Z):
            for j in range(1, X):
                basis_x_arrival(which, m, j).wait_recv()
                basis_spread(which, m, j)

    foreign = [(m, j) for j in range(X) for m in range(Z) if m or j]

    def basis_over_y(which):
        for m, j in foreign:
            for i in range(1, Y):
                basis_y(which, m, j, i, True).wait_recv()
                basis_mate(which, m, j, i).start()

    def basis_done(which):
        for m, j in foreign:
            for i in range(Y):
                basis_mate(which, m, j, i, True).wait_recv()

    in_rows, out_rows = w_in.shape[0] // Q, w_out.shape[0] // Q

    def place(item, s, q):
        if item == 0:
            return win_all.at[s, pl.ds(pl.multiple_of(q * in_rows, in_rows), in_rows)]
        return wout_all.at[s, pl.ds(pl.multiple_of(q * out_rows, out_rows), out_rows)]

    def down(m, q, item):
        at = place(item, (z + m) * X + x, q)
        return remote(at, at, wd_s.at[m, q, item], wd_r.at[m, q, item], ((z - 1) * X + x, t))

    def up(m, q, item):
        at = place(item, (z - m) * X + x, q)
        return remote(at, at, wu_s.at[m, q, item], wu_r.at[m, q, item], ((z + 1) * X + x, t))

    def aside(m, q, item, j):
        at = place(item, row(m) * X + x, q)
        return remote(at, at, wx_s.at[m, q, item, j], wx_r.at[m, q, item, j], (x_peer(j), t))

    def aside_arrival(m, q, item, j):
        at = place(item, row(m) * X + (x + X - j) % X, q)
        return remote(at, at, wx_s.at[m, q, item, j], wx_r.at[m, q, item, j], (x_peer(j), t))

    def down_arrival(m, q, item):
        at = place(item, (z + m) * X + x, q)
        return remote(at, at, wd_s.at[m - 1, q, item], wd_r.at[m - 1, q, item], (z_peer(1), t))

    def up_arrival(m, q, item):
        at = place(item, (z - m) * X + x, q)
        return remote(at, at, wu_s.at[m - 1, q, item], wu_r.at[m - 1, q, item], (z_peer(1), t))

    def goes_down(m):
        return (z >= 1) & (z + m <= Z - 1)

    def goes_up(m):
        return (z <= Z - 2) & (z - m >= 0)

    def z_settle(n):
        m, q = n // Q, n % Q

        @pl.when((n >= 0) & goes_down(m))
        def _():
            for item in range(2):
                down(m, q, item).wait_send()

        @pl.when((n >= 0) & goes_up(m))
        def _():
            for item in range(2):
                up(m, q, item).wait_send()

    def z_arrivals(n):
        m, q = n // Q, n % Q

        @pl.when((m >= 1) & (m <= Z - 1) & (z + m <= Z - 1))
        def _():
            for item in range(2):
                down_arrival(m, q, item).wait_recv()

        @pl.when((m >= 1) & (m <= Z - 1) & (z - m >= 0))
        def _():
            for item in range(2):
                up_arrival(m, q, item).wait_recv()

    def z_tick(n):
        m, q = n // Q, n % Q
        z_arrivals(n + AHEAD)
        z_settle(n - WINDOW)

        @pl.when(goes_down(m))
        def _():
            for item in range(2):
                down(m, q, item).start()

        @pl.when(goes_up(m))
        def _():
            for item in range(2):
                up(m, q, item).start()

    def x_settle(n):
        @pl.when(n >= 0)
        def _():
            for item in range(2):
                for j in range(1, X):
                    aside(n // Q, n % Q, item, j).wait_send()

    def x_tick(n):
        x_settle(n - WINDOW)
        for item in range(2):
            for j in range(1, X):
                aside(n // Q, n % Q, item, j).start()

    ticks = Z * Q
    passed = [0, 0]

    def loop(low, high, body):
        def step(n, carry):
            body(n)
            return carry

        if high > low:
            lax.fori_loop(low, high, step, 0)

    def pump(z_count, x_count):
        z_at, x_at = passed
        z_count, x_count = max(0, min(z_count, ticks - z_at)), max(0, min(x_count, ticks - x_at))
        both = min(z_count, x_count)

        def pair(n):
            z_tick(z_at + n)
            x_tick(x_at + n)

        loop(0, both, pair)
        loop(z_at + both, z_at + z_count, z_tick)
        loop(x_at + both, x_at + x_count, x_tick)
        passed[0], passed[1] = z_at + z_count, x_at + x_count
        assert passed[1] <= max(Q, passed[0] + AHEAD)

    def project(which, during):
        acc[which] = jnp.zeros(acc.shape[1:], jnp.float32)
        for i in range(chunks):
            for copy in fetch(which, i):
                copy.wait()
            span = pl.ds(i * chunk, chunk)
            whole = ball[which].reshape(h_buf.shape[2], -1)
            reduced = jnp.dot(h_buf[which, span], whole, preferred_element_type=jnp.float32)
            turned = reduced.T
            upper = turned.astype(jnp.bfloat16)
            lower = (turned - upper.astype(jnp.float32)).astype(jnp.bfloat16)
            block = c_buf[which, span]
            acc[which] += jnp.dot(upper, block, preferred_element_type=jnp.float32) + jnp.dot(
                lower, block, preferred_element_type=jnp.float32
            )
            during(i)
        part[which] = acc[which].astype(jnp.bfloat16).reshape(part.shape[1:])

    def part_x(which, j):
        return remote(
            part.at[which, pl.ds(0, Z), (x + j) % X],
            x_part.at[which, j],
            px_s.at[which, j],
            px_r.at[which, j],
            (x_peer(j), t),
        )

    def part_z(which, k):
        return remote(
            z_sum.at[which, (z + k) % Z],
            z_part.at[which, k],
            pz_s.at[which, k],
            pz_r.at[which, k],
            (z_peer(k), t),
        )

    def row_sum(which, to):
        value = acc[which, pl.ds(pl.multiple_of((to * X + x) * rr, rr), rr)]
        for j in range(1, X):
            value = value + x_part[which, j, to].astype(jnp.float32)
        return value

    def reduce_x(which):
        for j in range(1, X):
            part_x(which, j).wait_recv()
        for to in range(Z):
            z_sum[which, to] = row_sum(which, to).astype(jnp.bfloat16)
        for k in range(1, Z):
            part_z(which, k).start()

    def reduce_z(which):
        value = row_sum(which, z)
        for k in range(1, Z):
            part_z(which, k).wait_recv()
            value = value + z_part[which, k].astype(jnp.float32)
        return value

    def share(n):
        return remote(
            tot,
            tot_in.at[n],
            tot_s.at[n],
            tot_r.at[n],
            ((f + n // T) % F, (t + n % T) % T),
        )

    def dir_z(k):
        return remote(dall.at[f], dall.at[f], dz_s.at[k], dz_r.at[z], (z_peer(k), t))

    def dir_z_arrival(m):
        at = dall.at[row(m) * X + x]
        return remote(at, at, dz_s.at[m], dz_r.at[row(m)], (z_peer(1), t))

    def dir_x(m, j, arrival=False):
        at = dall.at[row(m) * X + ((x + X - j) % X if arrival else x)]
        return remote(at, at, dx_s.at[m, j], dx_r.at[m, j], (x_peer(j), t))

    def late(m):
        def each(q):
            for item in range(2):
                for j in range(1, X):
                    aside_arrival(m, q, item, j).wait_recv()

        loop(0, Q, each)

    def apply_own():
        direction = dall[:, 0].reshape(rank, cols)
        other = dall[:, 1].reshape(rank, cols)
        turned[...] = other.astype(jnp.float32).T.astype(jnp.bfloat16)
        step = jnp.dot(basis_in[...], direction, preferred_element_type=jnp.float32)
        step_in[...] = step
        new_in[...] = w_in[...] - 0.02 * step
        step = nt_dot(turned[...], basis_out[...])
        step_out[...] = step
        new_out[...] = w_out[...] - 0.02 * step

    def apply_row(m):
        direction = dall[:, 0].reshape(rank, cols)
        for j in range(X):
            s = row(m) * X + j
            span = pl.ds(pl.multiple_of(s * rows, rows), rows)
            step = jnp.dot(ball[0, s], direction, preferred_element_type=jnp.float32)
            copy_in[span] = (win_all[s].astype(jnp.float32) - 0.02 * step).astype(jnp.bfloat16)
            step = nt_dot(turned[...], ball[1, s])
            copy_out[:, span] = (wout_all[s].astype(jnp.float32) - 0.02 * step).astype(jnp.bfloat16)

    for which in range(2):
        basis_begin(which)
    pump(1, 1)
    basis_over_z(0)
    basis_over_z(1)
    pump(1, 1)
    basis_over_x(0)
    basis_over_x(1)
    pump(1, 1)
    basis_over_y(0)
    basis_done(0)

    def meanwhile(i):
        pump(1, 1)

    project(0, meanwhile)
    for j in range(1, X):
        part_x(0, j).start()
    basis_over_y(1)
    basis_done(1)

    def meanwhile(i):
        if i == 2:
            reduce_x(0)
        pump(1, 1)

    project(1, meanwhile)
    for j in range(1, X):
        part_x(1, j).start()
    pump(1, 1)
    reduce_x(1)
    pump(2, 2)
    projs = [reduce_z(which) for which in range(2)]
    square = sum(jnp.sum(value * value, axis=(0, 1), keepdims=True) for value in projs)
    tot[...] = jnp.broadcast_to(square, tot.shape)
    tot_in[0] = tot[...]
    loop(1, F * T, lambda n: share(n).start())
    pump(1, 1)
    loop(1, F * T, lambda n: share(n).wait())
    total = jnp.sum(jnp.sum(tot_in[...], axis=0), axis=0, keepdims=True)
    factor = (scale * lax.rsqrt(total + 1e-06))[0:1, 0:1]
    for which, (first, second, first_to, second_to) in enumerate(
        ((m_in, v_in, nm_in, nv_in), (m_out, v_out, nm_out, nv_out))
    ):
        scaled = factor * projs[which]
        first_new = 0.8 * first[...] + 0.2 * scaled
        second_new = 0.9 * second[...] + 0.1 * scaled * scaled
        first_to[...] = first_new
        second_to[...] = second_new
        dall[f, which] = (first_new / (jnp.sqrt(second_new) + 1e-08)).astype(jnp.bfloat16)
    for k in range(1, Z):
        dir_z(k).start()
    for j in range(1, X):
        dir_x(0, j).start()
    pump(2, 2)
    for m in range(1, Z):
        dir_z_arrival(m).wait_recv()
        for j in range(1, X):
            dir_x(m, j).start()
    pump(2, 2)
    for m in range(Z):
        for j in range(1, X):
            dir_x(m, j, True).wait_recv()
    apply_own()
    for m in range(Z):
        pump((m + 1) * Q - passed[1], (m + 1) * Q - passed[1])
        late(m)
        apply_row(m)
    pump(ticks, ticks)

    loop(ticks - WINDOW, ticks, z_settle)
    loop(ticks - WINDOW, ticks, x_settle)
    for which in range(2):
        for k in range(1, Z):
            basis_z(which, k).wait_send()
            part_z(which, k).wait_send()
        for j in range(1, X):
            part_x(which, j).wait_send()
            for m in range(Z):
                basis_x(which, m, j).wait_send()
        for m, j in foreign:
            for i in range(Y):
                if i:
                    basis_y(which, m, j, i).wait_send()
                basis_mate(which, m, j, i).wait_send()
    for k in range(1, Z):
        dir_z(k).wait_send()
    for m in range(Z):
        for j in range(1, X):
            dir_x(m, j).wait_send()


def flush(*refs):
    sources, targets, sems = refs[:10], refs[10:20], refs[20]
    copies = [pltpu.make_async_copy(a, b, sems.at[i]) for i, (a, b) in enumerate(zip(sources, targets))]
    for copy in copies:
        copy.start()
    for copy in copies:
        copy.wait()


def shards(mesh, h, cc, lo, oc, basis_in, basis_out, w_in, w_out, m_in, v_in, m_out, v_out):
    F, T = mesh.shape["fs"], mesh.shape["tp"]
    Z = next(n for n in range(1, F + 1) if F % n == 0 and n * n >= F)
    X, Y = F // Z, T // 2
    tokens, model = h.shape
    cols = cc.shape[1]
    rows, rank = basis_in.shape
    rr = m_in.shape[0]
    scale = math.sqrt(2.0 * rank * cols * T)
    chunks = max(1, tokens // 512)
    bf, f32 = jnp.bfloat16, jnp.float32
    hbm = pl.BlockSpec(memory_space=pl.ANY)
    vmem = pl.BlockSpec(memory_space=pltpu.VMEM)
    local = (w_in.shape, w_in.shape, (model, cols), m_in.shape, m_in.shape)
    local += (w_out.shape, w_out.shape, (cols, model), m_in.shape, m_in.shape)
    outs = tuple(jax.ShapeDtypeStruct(shape, bf if n in (2, 7) else f32) for n, shape in enumerate(local))

    def dma(*shape):
        return [pltpu.SemaphoreType.DMA(shape)] * 2

    results = pl.pallas_call(
        functools.partial(exchange, (F, T, Z, X, scale)),
        out_shape=outs,
        in_specs=[hbm] * 4 + [vmem] * 8,
        out_specs=(vmem,) * 10,
        scratch_shapes=[
            pltpu.VMEM((2, F, rows, rank), bf),
            pltpu.VMEM((F,) + w_in.shape, bf),
            pltpu.VMEM((F,) + w_out.shape, bf),
            pltpu.VMEM((F, 2, rr, cols), bf),
            pltpu.VMEM((cols, rank), bf),
            pltpu.VMEM((2, tokens, model), bf),
            pltpu.VMEM((2, tokens, cols), bf),
            pltpu.VMEM((2, rank, cols), f32),
            pltpu.VMEM((2, Z, X, rr, cols), bf),
            pltpu.VMEM((2, X, Z, rr, cols), bf),
            pltpu.VMEM((2, Z, rr, cols), bf),
            pltpu.VMEM((2, Z, rr, cols), bf),
            pltpu.VMEM((1, 128), f32),
            pltpu.VMEM((F * T, 1, 128), f32),
            pltpu.SemaphoreType.DMA((2, chunks, 2)),
            *dma(2, Z, X),
            *dma(2, Z),
            *dma(2, Z, X, Y),
            *dma(2, Z, X, Y),
            *dma(2, X),
            *dma(2, Z),
            *dma(F * T),
            *dma(Z, X),
            *dma(Z),
            *dma(Z, PIECES, 2),
            *dma(Z, PIECES, 2),
            *dma(Z, PIECES, 2, X),
        ],
        compiler_params=pltpu.CompilerParams(
            collective_id=0, has_side_effects=True, vmem_limit_bytes=VMEM_LIMIT
        ),
        name="exchange",
    )(h, cc, oc, lo, basis_in, basis_out, w_in, w_out, m_in, v_in, m_out, v_out)

    return pl.pallas_call(
        flush,
        out_shape=outs,
        in_specs=[hbm] * 10,
        out_specs=(hbm,) * 10,
        scratch_shapes=[pltpu.SemaphoreType.DMA((10,))],
        compiler_params=pltpu.CompilerParams(vmem_limit_bytes=FLUSH_LIMIT),
        name="flush",
    )(*results)


def solution(mesh):
    split, both = P("fs", None), P("fs", "tp")
    return jax.shard_map(
        functools.partial(shards, mesh),
        mesh=mesh,
        in_specs=(split, both, both, split, split, split, both, P("tp", "fs"), both, both, both, both),
        out_specs=(both, both, P(None, "tp"), both, both, P("tp", "fs"), P("tp", "fs"), P("tp", None), both, both),
        check_vma=False,
    )
```

time: 130 us -> 117 us (0.900)
  Pallas kernels: 129 us -> 108 us
  local copies, waits for them, and re-layouts: 0 us -> 7.52 us
    pallas_call x1, Pallas kernels: 118 us -> 105 us  [shards(): pl.pallas_call(functools.partial(exchange, (F, T, Z, X, scale)), out_shap...]
    unnamed x0 -> x16, local copies, waits for them, and re-layouts: none -> 7.52 us
    pallas_call x1, Pallas kernels: 10.8 us -> 3.35 us  [shards(): pl.pallas_call(flush, out_shape=outs, in_specs=[hbm] * 10, out_specs=(hbm...]
where the time goes in v1:
time: 117 us
  Pallas kernels  108 us (92%)
  local copies, waits for them, and re-layouts  7.52 us (6%)
    pallas_call x1, Pallas kernels, shards(): pl.pallas_call(functools.partial(exchange, (F, T, Z, X, scale)), out_shap...  105 us
    unnamed x16, local copies, waits for them, and re-layouts  7.52 us
    pallas_call x1, Pallas kernels, shards(): pl.pallas_call(flush, out_shape=outs, in_specs=[hbm] * 10, out_specs=(hbm...  3.35 us

profile of v1, /device:TPU:0, one launch (start us, length us, event | category | flops | bytes accessed | tf_op | source)
XLA Modules:
  0.0 116.7 jit_solution(9977516042933427612)
XLA Ops:
  0.6 0.0 copy-start
  0.7 1.1 copy-done
  1.7 0.0 copy-start.1
  1.7 1.1 copy-done.1
  2.8 0.0 copy-start.2
  2.8 0.9 copy-done.2
  3.7 0.0 copy-start.3
  3.7 0.9 copy-done.3
  4.6 0.0 copy-start.4
  4.6 0.9 copy-done.4
  5.5 0.0 copy-start.5
  5.5 0.9 copy-done.5
  6.4 0.0 copy-start.6
  6.4 0.9 copy-done.6
  7.3 0.0 copy-start.7
  7.3 0.9 copy-done.7
  8.2 105.0 %exchange.1 = (f32[256,640]{1,0:T(8,128)S(1)}, f32[256,640]{1,0:T(8,128)S(1)}, bf16[2048,640]{1,0:T(8,128)(2,1)S(1)}, f32[32,640]{1,0:T(8,128)S(1)}, f32[32,640]...) custom-call(bf16[2048,2048]{1,0:T(8,128)(2,1)} %h_hbm.1, ...), custom_call_target="tpu_custom_call" | custom-call | tf_op jit(solution)/shard_map/exchange/pallas_call | solution.py:560
  113.2 3.4 %flush.1 = (f32[256,640]{1,0:T(8,128)}, f32[256,640]{1,0:T(8,128)}, bf16[2048,640]{1,0:T(8,128)(2,1)}, f32[32,640]{1,0:T(8,128)}, f32[32,640]{1,0:T(8,128)}, /*i...) custom-call(f32[256,640]{1,0:T(8,128)S(1)} %get-tuple-element.20.ref, ...), custom_call_target="tpu_custom_call" | custom-call | tf_op jit(solution)/shard_map/flush/pallas_call | solution.py:600
Async XLA Ops:
  0.6 1.1 copy-start
  1.7 1.1 copy-start.1
  2.8 0.9 copy-start.2
  3.7 0.9 copy-start.3
  4.6 0.9 copy-start.4
  5.5 0.9 copy-start.5
  6.4 0.9 copy-start.6
  7.3 0.9 copy-start.7

commit v2 on v1

v2 whole, which is shorter than its diff:
```python
import functools
import math

import jax
import jax.numpy as jnp
from jax import lax
from jax.experimental import pallas as pl
from jax.experimental.pallas import tpu as pltpu
from jax.sharding import PartitionSpec as P

MESH = pl.DeviceIdType.MESH
VMEM_LIMIT = 42 * 1024 * 1024
FLUSH_LIMIT = 1024 * 1024
PIECES = 8
WINDOW = 3
AHEAD = 4
PLAN = [(3, 3), (3, 3), (2, 2), [(1, 1), (1, 1), (1, 1), (1, 1)], [(1, 1), (1, 1), (1, 1), (1, 1)], (2, 2), (3, 3), (2, 2), (3, 3), (3, 3)]


def nt_dot(left, right):
    return lax.dot_general(left, right, (((1,), (1,)), ((), ())), preferred_element_type=jnp.float32)


def exchange(
    dims,
    h_hbm,
    cc_hbm,
    oc_hbm,
    lo_hbm,
    basis_in,
    basis_out,
    w_in_hbm,
    w_out_hbm,
    m_in_hbm,
    v_in_hbm,
    m_out_hbm,
    v_out_hbm,
    step_in,
    new_in,
    copy_in,
    nm_in,
    nv_in,
    step_out,
    new_out,
    copy_out,
    nm_out,
    nv_out,
    ball,
    win_all,
    wout_all,
    dall,
    turned,
    h_buf,
    c_buf,
    acc,
    part,
    x_part,
    z_sum,
    z_part,
    tot,
    tot_in,
    w_in,
    w_out,
    m_in,
    v_in,
    m_out,
    v_out,
    in_sem,
    load_sem,
    b_s,
    bz_r,
    bx_r,
    by_r,
    bm_r,
    p_s,
    px_r,
    pz_r,
    tot_sem,
    d_s,
    dz_r,
    dx_r,
    w_s,
    wd_r,
    wu_r,
    wx_r,
):
    F, T, Z, X, scale = dims
    Y, Q = T // 2, PIECES
    f = lax.axis_index("fs")
    t = lax.axis_index("tp")
    z, x = f // X, f % X
    y, core = t // 2, t % 2
    mate = t + 1 - 2 * core
    turn = 1 - 2 * ((2 * z) // Z)
    chunks = in_sem.shape[1]
    chunk = h_buf.shape[1] // chunks
    rr, cols = m_in.shape
    rows, rank = ball.shape[2:]
    quarter = rows // T

    def remote(src, dst, send, recv, device):
        return pltpu.make_async_remote_copy(
            src_ref=src, dst_ref=dst, send_sem=send, recv_sem=recv, device_id=device, device_id_type=MESH
        )

    def settle(ref, sem):
        pltpu.make_async_copy(ref, ref, sem).wait()

    def z_peer(k):
        return ((z + k) % Z) * X + x

    def x_peer(j):
        return z * X + (x + j) % X

    def fetch(which, i):
        span = pl.ds(i * chunk, chunk)
        h_src, c_src = ((h_hbm, cc_hbm), (oc_hbm, lo_hbm))[which]
        return (
            pltpu.make_async_copy(h_src.at[span], h_buf.at[which, span], in_sem.at[which, i, 0]),
            pltpu.make_async_copy(c_src.at[span], c_buf.at[which, span], in_sem.at[which, i, 1]),
        )

    barrier = pltpu.get_barrier_semaphore()

    def greet(device):
        pl.semaphore_signal(barrier, inc=1, device_id=device, device_id_type=MESH)

    for k in range(1, Z):
        greet((z_peer(k), t))
    for j in range(1, X):
        greet((x_peer(j), t))
    for i in range(1, Y):
        greet((f, ((y + i) % Y) * 2 + core))
    greet((f, mate))
    loads = [
        pltpu.make_async_copy(src, dst, load_sem.at[n])
        for n, (src, dst) in enumerate(
            (
                (basis_in, ball.at[0, f]),
                (basis_out, ball.at[1, f]),
                (w_in_hbm, w_in),
                (w_out_hbm, w_out),
                (m_in_hbm, m_in),
                (v_in_hbm, v_in),
                (m_out_hbm, m_out),
                (v_out_hbm, v_out),
            )
        )
    ]
    for copy in loads:
        copy.start()
    for which in range(2):
        for i in range(chunks):
            for copy in fetch(which, i):
                copy.start()
    own = pl.ds(pl.multiple_of(t * quarter, quarter), quarter)
    for copy in loads:
        copy.wait()
    win_all[f] = w_in[...].astype(jnp.bfloat16)
    wout_all[f] = w_out[...].astype(jnp.bfloat16)
    pl.semaphore_wait(barrier, (Z - 1) + (X - 1) + (Y - 1) + 1)

    def row(m):
        return (z + turn * m + Z) % Z

    def basis_at(which, m, j, part_of):
        s = row(m) * X + (x + X - j) % X
        return ball.at[which, s, pl.ds(pl.multiple_of(part_of * quarter, quarter), quarter)]

    def basis_z(which, k):
        at = ball.at[which, f, own]
        return remote(at, at, b_s.at[0], bz_r.at[which, z], (z_peer(k), t))

    def basis_z_arrival(which, m):
        at = basis_at(which, m, 0, t)
        return remote(at, at, b_s.at[0], bz_r.at[which, row(m)], (z_peer(1), t))

    def basis_x(which, m, j):
        at = basis_at(which, m, 0, t)
        return remote(at, at, b_s.at[1], bx_r.at[which, m, j - 1], (x_peer(j), t))

    def basis_x_arrival(which, m, j):
        at = basis_at(which, m, j, t)
        return remote(at, at, b_s.at[1], bx_r.at[which, m, j - 1], (x_peer(j), t))

    def basis_y(which, m, j, i):
        at = basis_at(which, m, j, t)
        return remote(at, at, b_s.at[2], by_r.at[which], (f, ((y + i) % Y) * 2 + core))

    def basis_mate(which, m, j, i):
        at = basis_at(which, m, j, ((y + Y - i) % Y) * 2 + core)
        return remote(at, at, b_s.at[3], bm_r.at[which], (f, mate))

    def basis_begin(which):
        for k in range(1, Z):
            basis_z(which, k).start()
        for j in range(1, X):
            basis_x(which, 0, j).start()

    def basis_spread(which, m, j):
        for i in range(1, Y):
            basis_y(which, m, j, i).start()
        basis_mate(which, m, j, 0).start()

    def basis_over_z(which):
        for m in range(1, Z):
            basis_z_arrival(which, m).wait_recv()
            for j in range(1, X):
                basis_x(which, m, j).start()
            basis_spread(which, m, 0)

    def basis_over_x(which):
        for m in range(Z):
            for j in range(1, X):
                basis_x_arrival(which, m, j).wait_recv()
                basis_spread(which, m, j)

    foreign = [(m, j) for j in range(X) for m in range(Z) if m or j]

    def basis_bytes(whiches, shares):
        return ball.at[whiches, pl.ds(0, F - 1), pl.ds(0, shares * quarter)]

    def basis_over_y(which):
        if Y > 1:
            settle(basis_bytes(which, Y - 1), by_r.at[which])
        for m, j in foreign:
            for i in range(1, Y):
                basis_mate(which, m, j, i).start()

    def basis_done(which):
        settle(basis_bytes(which, Y), bm_r.at[which])

    in_rows, out_rows = 2 * w_in.shape[0] // Q, 2 * w_out.shape[0] // Q

    def place(item, s, q):
        if item == 0:
            return win_all.at[s, pl.ds(pl.multiple_of((q // 2) * in_rows, in_rows), in_rows)]
        return wout_all.at[s, pl.ds(pl.multiple_of((q // 2) * out_rows, out_rows), out_rows)]

    def turns(q, body):
        for item in range(2):

            @pl.when(q % 2 == item)
            def _(item=item):
                body(item)

    def down(n, item):
        m, q = n // Q, n % Q
        at = place(item, (z + m) * X + x, q)
        return remote(at, at, w_s.at[0, n % WINDOW, 0], wd_r.at[m, q], ((z - 1) * X + x, t))

    def up(n, item):
        m, q = n // Q, n % Q
        at = place(item, (z - m) * X + x, q)
        return remote(at, at, w_s.at[1, n % WINDOW, 0], wu_r.at[m, q], ((z + 1) * X + x, t))

    def aside(n, item, j):
        m, q = n // Q, n % Q
        at = place(item, row(m) * X + x, q)
        return remote(
            at, at, w_s.at[2, n % WINDOW, j - 1], wx_r.at[m, q, j - 1], (x_peer(j), t)
        )

    def aside_arrival(n, item, j):
        m, q = n // Q, n % Q
        at = place(item, row(m) * X + (x + X - j) % X, q)
        return remote(at, at, w_s.at[2, 0, j - 1], wx_r.at[m, q, j - 1], (x_peer(j), t))

    def down_arrival(n, item):
        m, q = n // Q, n % Q
        at = place(item, (z + m) * X + x, q)
        return remote(at, at, w_s.at[0, 0, 0], wd_r.at[m - 1, q], (z_peer(1), t))

    def up_arrival(n, item):
        m, q = n // Q, n % Q
        at = place(item, (z - m) * X + x, q)
        return remote(at, at, w_s.at[1, 0, 0], wu_r.at[m - 1, q], (z_peer(1), t))

    def goes_down(m):
        return (z >= 1) & (z + m <= Z - 1)

    def goes_up(m):
        return (z <= Z - 2) & (z - m >= 0)

    def z_settle(n):
        m, q = n // Q, n % Q

        @pl.when((n >= 0) & goes_down(m))
        def _():
            turns(q, lambda item: down(n, item).wait_send())

        @pl.when((n >= 0) & goes_up(m))
        def _():
            turns(q, lambda item: up(n, item).wait_send())

    def z_arrivals(n):
        m, q = n // Q, n % Q

        @pl.when((m >= 1) & (m <= Z - 1) & (z + m <= Z - 1))
        def _():
            turns(q, lambda item: down_arrival(n, item).wait_recv())

        @pl.when((m >= 1) & (m <= Z - 1) & (z - m >= 0))
        def _():
            turns(q, lambda item: up_arrival(n, item).wait_recv())

    def z_tick(n):
        m, q = n // Q, n % Q
        z_arrivals(n + AHEAD)
        z_settle(n - WINDOW)

        @pl.when(goes_down(m))
        def _():
            turns(q, lambda item: down(n, item).start())

        @pl.when(goes_up(m))
        def _():
            turns(q, lambda item: up(n, item).start())

    def x_settle(n):
        @pl.when(n >= 0)
        def _():
            for j in range(1, X):
                turns(n % Q, lambda item: aside(n, item, j).wait_send())

    def x_tick(n):
        x_settle(n - WINDOW)
        for j in range(1, X):
            turns(n % Q, lambda item: aside(n, item, j).start())

    ticks = Z * Q
    passed = [0, 0]

    def loop(low, high, body):
        def step(n, carry):
            body(n)
            return carry

        if high > low:
            lax.fori_loop(low, high, step, 0)

    def pump(z_count, x_count):
        z_at, x_at = passed
        z_count, x_count = max(0, min(z_count, ticks - z_at)), max(0, min(x_count, ticks - x_at))
        both = min(z_count, x_count)

        def pair(n):
            z_tick(z_at + n)
            x_tick(x_at + n)

        loop(0, both, pair)
        loop(z_at + both, z_at + z_count, z_tick)
        loop(x_at + both, x_at + x_count, x_tick)
        passed[0], passed[1] = z_at + z_count, x_at + x_count
        assert passed[1] <= max(Q, passed[0] + AHEAD)

    def project(which, during):
        acc[which] = jnp.zeros(acc.shape[1:], jnp.float32)
        for i in range(chunks):
            for copy in fetch(which, i):
                copy.wait()
            span = pl.ds(i * chunk, chunk)
            whole = ball[which].reshape(h_buf.shape[2], -1)
            reduced = jnp.dot(h_buf[which, span], whole, preferred_element_type=jnp.float32)
            turned_bf = reduced.T.astype(jnp.bfloat16)
            acc[which] += jnp.dot(turned_bf, c_buf[which, span], preferred_element_type=jnp.float32)
            during(i)
        part[which] = acc[which].astype(jnp.bfloat16).reshape(part.shape[1:])

    def part_x(which, j):
        return remote(
            part.at[which, pl.ds(0, Z), (x + j) % X],
            x_part.at[which, j],
            p_s.at[0],
            px_r.at[which, j - 1],
            (x_peer(j), t),
        )

    def part_z(which, k):
        return remote(
            z_sum.at[which, (z + k) % Z], z_part.at[which, k], p_s.at[1], pz_r.at[which], (z_peer(k), t)
        )

    def row_sum(which, to):
        value = acc[which, pl.ds(pl.multiple_of((to * X + x) * rr, rr), rr)]
        for j in range(1, X):
            value = value + x_part[which, j, to].astype(jnp.float32)
        return value

    def reduce_x(which):
        for j in range(1, X):
            part_x(which, j).wait_recv()
        for to in range(Z):
            z_sum[which, to] = row_sum(which, to).astype(jnp.bfloat16)
        for k in range(1, Z):
            part_z(which, k).start()

    def reduce_z(which):
        value = row_sum(which, z)
        settle(z_part.at[which, pl.ds(1, Z - 1)], pz_r.at[which])
        for k in range(1, Z):
            value = value + z_part[which, k].astype(jnp.float32)
        return value

    def share(n):
        return remote(
            tot,
            tot_in.at[n],
            tot_sem.at[0],
            tot_sem.at[1],
            ((f + n // T) % F, (t + n % T) % T),
        )

    def dir_z(k):
        return remote(dall.at[f], dall.at[f], d_s.at[0], dz_r.at[z], (z_peer(k), t))

    def dir_z_arrival(m):
        at = dall.at[row(m) * X + x]
        return remote(at, at, d_s.at[0], dz_r.at[row(m)], (z_peer(1), t))

    def dir_x(m, j):
        at = dall.at[row(m) * X + x]
        return remote(at, at, d_s.at[1], dx_r.at[0], (x_peer(j), t))

    def late(m):
        def each(q):
            for j in range(1, X):
                turns(q, lambda item: aside_arrival(m * Q + q, item, j).wait_recv())

        loop(0, Q, each)

    def apply_own():
        direction = dall[:, 0].reshape(rank, cols)
        other = dall[:, 1].reshape(rank, cols)
        turned[...] = other.astype(jnp.float32).T.astype(jnp.bfloat16)
        step = jnp.dot(ball[0, f], direction, preferred_element_type=jnp.float32)
        step_in[...] = step
        new_in[...] = w_in[...] - 0.02 * step
        step = nt_dot(turned[...], ball[1, f])
        step_out[...] = step
        new_out[...] = w_out[...] - 0.02 * step

    def apply_row(m):
        direction = dall[:, 0].reshape(rank, cols)
        for j in range(X):
            s = row(m) * X + j
            span = pl.ds(pl.multiple_of(s * rows, rows), rows)
            step = jnp.dot(ball[0, s], direction, preferred_element_type=jnp.float32)
            copy_in[span] = (win_all[s].astype(jnp.float32) - 0.02 * step).astype(jnp.bfloat16)
            step = nt_dot(turned[...], ball[1, s])
            copy_out[:, span] = (wout_all[s].astype(jnp.float32) - 0.02 * step).astype(jnp.bfloat16)

    for which in range(2):
        basis_begin(which)
    pump(*PLAN[0])
    basis_over_z(0)
    basis_over_z(1)
    pump(*PLAN[1])
    basis_over_x(0)
    basis_over_x(1)
    pump(*PLAN[2])
    basis_over_y(0)
    basis_done(0)
    project(0, lambda i: pump(*PLAN[3][i]))
    for j in range(1, X):
        part_x(0, j).start()
    basis_over_y(1)
    basis_done(1)

    def meanwhile(i):
        if i == 2:
            reduce_x(0)
        pump(*PLAN[4][i])

    project(1, meanwhile)
    for j in range(1, X):
        part_x(1, j).start()
    pump(*PLAN[5])
    reduce_x(1)
    pump(*PLAN[6])
    projs = [reduce_z(which) for which in range(2)]
    square = sum(jnp.sum(value * value, axis=(0, 1), keepdims=True) for value in projs)
    tot[...] = jnp.broadcast_to(square, tot.shape)
    tot_in[0] = tot[...]
    loop(1, F * T, lambda n: share(n).start())
    pump(*PLAN[7])
    for sem in range(2):
        settle(tot_in.at[pl.ds(1, F * T - 1)], tot_sem.at[sem])
    total = jnp.sum(jnp.sum(tot_in[...], axis=0), axis=0, keepdims=True)
    factor = (scale * lax.rsqrt(total + 1e-06))[0:1, 0:1]
    for which, (first, second, first_to, second_to) in enumerate(
        ((m_in, v_in, nm_in, nv_in), (m_out, v_out, nm_out, nv_out))
    ):
        scaled = factor * projs[which]
        first_new = 0.8 * first[...] + 0.2 * scaled
        second_new = 0.9 * second[...] + 0.1 * scaled * scaled
        first_to[...] = first_new
        second_to[...] = second_new
        dall[f, which] = (first_new / (jnp.sqrt(second_new) + 1e-08)).astype(jnp.bfloat16)
    for k in range(1, Z):
        dir_z(k).start()
    for j in range(1, X):
        dir_x(0, j).start()
    pump(*PLAN[8])
    for m in range(1, Z):
        dir_z_arrival(m).wait_recv()
        for j in range(1, X):
            dir_x(m, j).start()
    pump(*PLAN[9])
    settle(dall.at[pl.ds(0, Z * (X - 1))], dx_r.at[0])
    apply_own()
    for m in range(Z):
        pump((m + 1) * Q - passed[1], (m + 1) * Q - passed[1])
        late(m)
        apply_row(m)
    pump(ticks, ticks)

    loop(ticks - WINDOW, ticks, z_settle)
    loop(ticks - WINDOW, ticks, x_settle)
    both = pl.ds(0, 2)
    settle(ball.at[both, pl.ds(0, Z - 1), pl.ds(0, quarter)], b_s.at[0])
    settle(ball.at[both, pl.ds(0, Z * (X - 1)), pl.ds(0, quarter)], b_s.at[1])
    if Y > 1:
        settle(basis_bytes(both, Y - 1), b_s.at[2])
    settle(basis_bytes(both, Y), b_s.at[3])
    settle(part.at[both, pl.ds(0, Z), pl.ds(0, X - 1)], p_s.at[0])
    settle(z_sum.at[both, pl.ds(0, Z - 1)], p_s.at[1])
    settle(dall.at[pl.ds(0, Z - 1)], d_s.at[0])
    settle(dall.at[pl.ds(0, Z * (X - 1))], d_s.at[1])


def flush(*refs):
    sources, targets, sems = refs[:10], refs[10:20], refs[20]
    copies = [pltpu.make_async_copy(a, b, sems.at[i]) for i, (a, b) in enumerate(zip(sources, targets))]
    for copy in copies:
        copy.start()
    for copy in copies:
        copy.wait()


def shards(mesh, h, cc, lo, oc, basis_in, basis_out, w_in, w_out, m_in, v_in, m_out, v_out):
    F, T = mesh.shape["fs"], mesh.shape["tp"]
    Z = next(n for n in range(1, F + 1) if F % n == 0 and n * n >= F)
    X, Y = F // Z, T // 2
    tokens, model = h.shape
    cols = cc.shape[1]
    rows, rank = basis_in.shape
    rr = m_in.shape[0]
    scale = math.sqrt(2.0 * rank * cols * T)
    chunks = max(1, tokens // 512)
    bf, f32 = jnp.bfloat16, jnp.float32
    hbm = pl.BlockSpec(memory_space=pltpu.HBM)
    anywhere = pl.BlockSpec(memory_space=pl.ANY)
    vmem = pl.BlockSpec(memory_space=pltpu.VMEM)
    local = (w_in.shape, w_in.shape, (model, cols), m_in.shape, m_in.shape)
    local += (w_out.shape, w_out.shape, (cols, model), m_in.shape, m_in.shape)
    outs = tuple(jax.ShapeDtypeStruct(shape, bf if n in (2, 7) else f32) for n, shape in enumerate(local))

    dma = pltpu.SemaphoreType.DMA
    results = pl.pallas_call(
        functools.partial(exchange, (F, T, Z, X, scale)),
        out_shape=outs,
        in_specs=[hbm] * 12,
        out_specs=(vmem,) * 10,
        scratch_shapes=[
            pltpu.VMEM((2, F, rows, rank), bf),
            pltpu.VMEM((F,) + w_in.shape, bf),
            pltpu.VMEM((F,) + w_out.shape, bf),
            pltpu.VMEM((F, 2, rr, cols), bf),
            pltpu.VMEM((cols, rank), bf),
            pltpu.VMEM((2, tokens, model), bf),
            pltpu.VMEM((2, tokens, cols), bf),
            pltpu.VMEM((2, rank, cols), f32),
            pltpu.VMEM((2, Z, X, rr, cols), bf),
            pltpu.VMEM((2, X, Z, rr, cols), bf),
            pltpu.VMEM((2, Z, rr, cols), bf),
            pltpu.VMEM((2, Z, rr, cols), bf),
            pltpu.VMEM((1, 128), f32),
            pltpu.VMEM((F * T, 1, 128), f32),
            pltpu.VMEM(w_in.shape, f32),
            pltpu.VMEM(w_out.shape, f32),
            *[pltpu.VMEM(m_in.shape, f32)] * 4,
            dma((2, chunks, 2)),
            dma((8,)),
            dma((4,)),
            dma((2, Z)),
            dma((2, Z, X - 1)),
            dma((2,)),
            dma((2,)),
            dma((2,)),
            dma((2, X - 1)),
            dma((2,)),
            dma((2,)),
            dma((2,)),
            dma((Z,)),
            dma((1,)),
            dma((3, WINDOW, X - 1)),
            dma((Z - 1, PIECES)),
            dma((Z - 1, PIECES)),
            dma((Z, PIECES, X - 1)),
        ],
        compiler_params=pltpu.CompilerParams(
            collective_id=0, has_side_effects=True, vmem_limit_bytes=VMEM_LIMIT
        ),
        name="exchange",
    )(
        *(
            pltpu.with_memory_space_constraint(array, pltpu.HBM)
            for array in (h, cc, oc, lo, basis_in, basis_out, w_in, w_out, m_in, v_in, m_out, v_out)
        )
    )

    return pl.pallas_call(
        flush,
        out_shape=outs,
        in_specs=[anywhere] * 10,
        out_specs=(anywhere,) * 10,
        scratch_shapes=[pltpu.SemaphoreType.DMA((10,))],
        compiler_params=pltpu.CompilerParams(vmem_limit_bytes=FLUSH_LIMIT),
        name="flush",
    )(*results)


def solution(mesh):
    split, both = P("fs", None), P("fs", "tp")
    return jax.shard_map(
        functools.partial(shards, mesh),
        mesh=mesh,
        in_specs=(split, both, both, split, split, split, both, P("tp", "fs"), both, both, both, both),
        out_specs=(both, both, P(None, "tp"), both, both, P("tp", "fs"), P("tp", "fs"), P("tp", None), both, both),
        check_vma=False,
    )
```

time: 117 us -> 96 us (0.82)
  Pallas kernels: 108 us -> 95.2 us
  local copies, waits for them, and re-layouts: 7.52 us -> 0 us
    pallas_call x1, Pallas kernels: 105 us -> 91.8 us  [shards(): pl.pallas_call(functools.partial(exchange, (F, T, Z, X, scale)), out_shap...]
    unnamed x16 -> x0, local copies, waits for them, and re-layouts: 7.52 us -> none
where the time goes in v2:
time: 96 us; the launch traced here: 95.8 us
  Pallas kernels  95.2 us (99%)
    pallas_call x1, Pallas kernels, shards(): pl.pallas_call(functools.partial(exchange, (F, T, Z, X, scale)), out_shap...  91.8 us
    pallas_call x1, Pallas kernels, shards(): pl.pallas_call(flush, out_shape=outs, in_specs=[anywhere] * 10, out_specs...  3.35 us

profile of v2, /device:TPU:0, one launch (start us, length us, event | category | flops | bytes accessed | tf_op | source)
XLA Modules:
  0.0 95.8 jit_solution(5415216467649911289)
XLA Ops:
  0.6 91.8 %exchange.1 = (f32[256,640]{1,0:T(8,128)S(1)}, f32[256,640]{1,0:T(8,128)S(1)}, bf16[2048,640]{1,0:T(8,128)(2,1)S(1)}, f32[32,640]{1,0:T(8,128)S(1)}, f32[32,640]...) custom-call(bf16[2048,2048]{1,0:T(8,128)(2,1)} %h_hbm.1, ...), custom_call_target="tpu_custom_call" | custom-call | tf_op jit(solution)/shard_map/exchange/pallas_call | solution.py:560
  92.5 3.4 %flush.1 = (f32[256,640]{1,0:T(8,128)}, f32[256,640]{1,0:T(8,128)}, bf16[2048,640]{1,0:T(8,128)(2,1)}, f32[32,640]{1,0:T(8,128)}, f32[32,640]{1,0:T(8,128)}, /*i...) custom-call(f32[256,640]{1,0:T(8,128)S(1)} %get-tuple-element.20.ref, ...), custom_call_target="tpu_custom_call" | custom-call | tf_op jit(solution)/shard_map/flush/pallas_call | solution.py:613

commit v3 on v2

--- a/solution.py
+++ b/solution.py
@@ -12,9 +12,10 @@
 VMEM_LIMIT = 42 * 1024 * 1024
 FLUSH_LIMIT = 1024 * 1024
 PIECES = 8
+DOUBLED = 2
 WINDOW = 3
-AHEAD = 4
-PLAN = [(3, 3), (3, 3), (2, 2), [(1, 1), (1, 1), (1, 1), (1, 1)], [(1, 1), (1, 1), (1, 1), (1, 1)], (2, 2), (3, 3), (2, 2), (3, 3), (3, 3)]
+AHEAD = 6
+PLAN = [(3, 3), (3, 3), (3, 3), [(1, 1)] * 4, [(1, 1), (0, 0)] * 2, (2, 1), (3, 2), (4, 3), (6, 5), (8, 6)]
 
 
 def nt_dot(left, right):
@@ -85,7 +86,8 @@
     wx_r,
 ):
     F, T, Z, X, scale = dims
-    Y, Q = T // 2, PIECES
+    Y, Q, D = T // 2, PIECES, DOUBLED
+    R = Q + D * (X - 1)
     f = lax.axis_index("fs")
     t = lax.axis_index("tp")
     z, x = f // X, f % X
@@ -244,37 +246,39 @@
             def _(item=item):
                 body(item)
 
+    def z_piece(n):
+        m, r = n // R, n % R
+        extra = r // Q
+        j = extra * (1 + r // D - Q // D)
+        return m, (x + X - j) % X, (1 - extra) * r + extra * (Q - D + r % D)
+
     def down(n, item):
-        m, q = n // Q, n % Q
-        at = place(item, (z + m) * X + x, q)
-        return remote(at, at, w_s.at[0, n % WINDOW, 0], wd_r.at[m, q], ((z - 1) * X + x, t))
+        m, c, q = z_piece(n)
+        at = place(item, (z + m) * X + c, q)
+        return remote(at, at, w_s.at[0, n % WINDOW, 0], wd_r.at[n], ((z - 1) * X + x, t))
 
     def up(n, item):
-        m, q = n // Q, n % Q
-        at = place(item, (z - m) * X + x, q)
-        return remote(at, at, w_s.at[1, n % WINDOW, 0], wu_r.at[m, q], ((z + 1) * X + x, t))
-
-    def aside(n, item, j):
-        m, q = n // Q, n % Q
+        m, c, q = z_piece(n)
+        at = place(item, (z - m) * X + c, q)
+        return remote(at, at, w_s.at[1, n % WINDOW, 0], wu_r.at[n], ((z + 1) * X + x, t))
+
+    def aside(n, m, q, item, j):
         at = place(item, row(m) * X + x, q)
-        return remote(
-            at, at, w_s.at[2, n % WINDOW, j - 1], wx_r.at[m, q, j - 1], (x_peer(j), t)
-        )
-
-    def aside_arrival(n, item, j):
-        m, q = n // Q, n % Q
+        return remote(at, at, w_s.at[2, n % WINDOW, j - 1], wx_r.at[n, j - 1], (x_peer(j), t))
+
+    def aside_arrival(n, m, q, item, j):
         at = place(item, row(m) * X + (x + X - j) % X, q)
-        return remote(at, at, w_s.at[2, 0, j - 1], wx_r.at[m, q, j - 1], (x_peer(j), t))
+        return remote(at, at, w_s.at[2, 0, j - 1], wx_r.at[n, j - 1], (x_peer(1), t))
 
     def down_arrival(n, item):
-        m, q = n // Q, n % Q
-        at = place(item, (z + m) * X + x, q)
-        return remote(at, at, w_s.at[0, 0, 0], wd_r.at[m - 1, q], (z_peer(1), t))
+        m, c, q = z_piece(n)
+        at = place(item, (z + m) * X + c, q)
+        return remote(at, at, w_s.at[0, 0, 0], wd_r.at[n - R], (z_peer(1), t))
 
     def up_arrival(n, item):
-        m, q = n // Q, n % Q
-        at = place(item, (z - m) * X + x, q)
-        return remote(at, at, w_s.at[1, 0, 0], wu_r.at[m - 1, q], (z_peer(1), t))
+        m, c, q = z_piece(n)
+        at = place(item, (z - m) * X + c, q)
+        return remote(at, at, w_s.at[1, 0, 0], wu_r.at[n - R], (z_peer(1), t))
 
     def goes_down(m):
         return (z >= 1) & (z + m <= Z - 1)
@@ -283,52 +287,79 @@
         return (z <= Z - 2) & (z - m >= 0)
 
     def z_settle(n):
-        m, q = n // Q, n % Q
+        m = n // R
 
         @pl.when((n >= 0) & goes_down(m))
         def _():
-            turns(q, lambda item: down(n, item).wait_send())
+            turns(n % R, lambda item: down(n, item).wait_send())
 
         @pl.when((n >= 0) & goes_up(m))
         def _():
-            turns(q, lambda item: up(n, item).wait_send())
+            turns(n % R, lambda item: up(n, item).wait_send())
 
     def z_arrivals(n):
-        m, q = n // Q, n % Q
+        m = n // R
 
         @pl.when((m >= 1) & (m <= Z - 1) & (z + m <= Z - 1))
         def _():
-            turns(q, lambda item: down_arrival(n, item).wait_recv())
+            turns(n % R, lambda item: down_arrival(n, item).wait_recv())
 
         @pl.when((m >= 1) & (m <= Z - 1) & (z - m >= 0))
         def _():
-            turns(q, lambda item: up_arrival(n, item).wait_recv())
+            turns(n % R, lambda item: up_arrival(n, item).wait_recv())
 
     def z_tick(n):
-        m, q = n // Q, n % Q
+        m, r = n // R, n % R
         z_arrivals(n + AHEAD)
         z_settle(n - WINDOW)
 
+        @pl.when((m == 0) & (r >= Q))
+        def _():
+            e = r % D
+            turns(e, lambda item: aside_arrival(e, 0, Q - D + e, item, 1 + r // D - Q // D).wait_recv())
+
         @pl.when(goes_down(m))
         def _():
-            turns(q, lambda item: down(n, item).start())
+            turns(r, lambda item: down(n, item).start())
 
         @pl.when(goes_up(m))
         def _():
-            turns(q, lambda item: up(n, item).start())
+            turns(r, lambda item: up(n, item).start())
+
+    def x_first(n):
+        return 0, (n + Q - D) % Q
+
+    def x_later(n):
+        return 1 + (n - Q) // (Q - D), (n - Q) % (Q - D)
 
     def x_settle(n):
-        @pl.when(n >= 0)
-        def _():
-            for j in range(1, X):
-                turns(n % Q, lambda item: aside(n, item, j).wait_send())
-
-    def x_tick(n):
+        for j in range(1, X):
+
+            @pl.when((n >= 0) & (n < Q))
+            def _(j=j):
+                m, q = x_first(n)
+                turns(q, lambda item: aside(n, m, q, item, j).wait_send())
+
+            @pl.when(n >= Q)
+            def _(j=j):
+                m, q = x_later(n)
+                turns(q, lambda item: aside(n, m, q, item, j).wait_send())
+
+    def x_start(n, m, q):
         x_settle(n - WINDOW)
         for j in range(1, X):
-            turns(n % Q, lambda item: aside(n, item, j).start())
-
-    ticks = Z * Q
+            turns(q, lambda item: aside(n, m, q, item, j).start())
+
+    def x_tick(n):
+        @pl.when(n < Q)
+        def _():
+            x_start(n, *x_first(n))
+
+        @pl.when(n >= Q)
+        def _():
+            x_start(n, *x_later(n))
+
+    z_ticks, x_ticks = Z * R, Q + (Z - 1) * (Q - D)
     passed = [0, 0]
 
     def loop(low, high, body):
@@ -341,18 +372,25 @@
 
     def pump(z_count, x_count):
         z_at, x_at = passed
-        z_count, x_count = max(0, min(z_count, ticks - z_at)), max(0, min(x_count, ticks - x_at))
-        both = min(z_count, x_count)
+        z_count, x_count = max(0, min(z_count, z_ticks - z_at)), max(0, min(x_count, x_ticks - x_at))
+        lead = max(0, z_count - x_count)
+
+        def ready(n):
+            m, q = x_later(x_at + n)
+            return x_at + n < Q or m * R + q < min(z_at + min(z_count, lead + n + 1) + AHEAD, z_ticks + R)
+
+        x_count = next((n for n in range(x_count) if not ready(n)), x_count)
+        both = min(z_count - lead, x_count)
 
         def pair(n):
-            z_tick(z_at + n)
+            z_tick(z_at + lead + n)
             x_tick(x_at + n)
 
+        loop(z_at, z_at + lead, z_tick)
         loop(0, both, pair)
-        loop(z_at + both, z_at + z_count, z_tick)
+        loop(z_at + lead + both, z_at + z_count, z_tick)
         loop(x_at + both, x_at + x_count, x_tick)
         passed[0], passed[1] = z_at + z_count, x_at + x_count
-        assert passed[1] <= max(Q, passed[0] + AHEAD)
 
     def project(which, during):
         acc[which] = jnp.zeros(acc.shape[1:], jnp.float32)
@@ -423,11 +461,12 @@
         return remote(at, at, d_s.at[1], dx_r.at[0], (x_peer(j), t))
 
     def late(m):
-        def each(q):
+        def each(n):
+            at = x_later(n) if m else x_first(n)
             for j in range(1, X):
-                turns(q, lambda item: aside_arrival(m * Q + q, item, j).wait_recv())
-
-        loop(0, Q, each)
+                turns(at[1], lambda item: aside_arrival(n, *at, item, j).wait_recv())
+
+        loop(D if m == 0 else Q + (m - 1) * (Q - D), Q + m * (Q - D), each)
 
     def apply_own():
         direction = dall[:, 0].reshape(rank, cols)
@@ -461,16 +500,16 @@
     pump(*PLAN[2])
     basis_over_y(0)
     basis_done(0)
-    project(0, lambda i: pump(*PLAN[3][i]))
+    project(0, lambda i: pump(*PLAN[3][i % 4]))
     for j in range(1, X):
         part_x(0, j).start()
     basis_over_y(1)
     basis_done(1)
 
     def meanwhile(i):
-        if i == 2:
+        if i == min(2, chunks - 1):
             reduce_x(0)
-        pump(*PLAN[4][i])
+        pump(*PLAN[4][i % 4])
 
     project(1, meanwhile)
     for j in range(1, X):
@@ -510,13 +549,14 @@
     settle(dall.at[pl.ds(0, Z * (X - 1))], dx_r.at[0])
     apply_own()
     for m in range(Z):
-        pump((m + 1) * Q - passed[1], (m + 1) * Q - passed[1])
+        z_left, x_left = min(z_ticks, (m + 1) * R) - passed[0], Q + m * (Q - D) - passed[1]
+        pump(z_left, x_left)
+        assert passed[1] >= Q + m * (Q - D)
         late(m)
         apply_row(m)
-    pump(ticks, ticks)
-
-    loop(ticks - WINDOW, ticks, z_settle)
-    loop(ticks - WINDOW, ticks, x_settle)
+
+    loop(z_ticks - WINDOW, z_ticks, z_settle)
+    loop(x_ticks - WINDOW, x_ticks, x_settle)
     both = pl.ds(0, 2)
     settle(ball.at[both, pl.ds(0, Z - 1), pl.ds(0, quarter)], b_s.at[0])
     settle(ball.at[both, pl.ds(0, Z * (X - 1)), pl.ds(0, quarter)], b_s.at[1])
@@ -595,9 +635,9 @@
             dma((Z,)),
             dma((1,)),
             dma((3, WINDOW, X - 1)),
-            dma((Z - 1, PIECES)),
-            dma((Z - 1, PIECES)),
-            dma((Z, PIECES, X - 1)),
+            dma(((Z - 1) * (PIECES + DOUBLED * (X - 1)),)),
+            dma(((Z - 1) * (PIECES + DOUBLED * (X - 1)),)),
+            dma((PIECES + (Z - 1) * (PIECES - DOUBLED), X - 1)),
         ],
         compiler_params=pltpu.CompilerParams(
             collective_id=0, has_side_effects=True, vmem_limit_bytes=VMEM_LIMIT

time: 96 us -> 95.9 us (level)
  no operation moved by 1% of the time
where the time goes in v3:
time: 95.9 us; the launch traced here: 95.7 us
  Pallas kernels  95.1 us (99%)
    pallas_call x1, Pallas kernels, shards(): pl.pallas_call(functools.partial(exchange, (F, T, Z, X, scale)), out_shap...  91.7 us
    pallas_call x1, Pallas kernels, shards(): pl.pallas_call(flush, out_shape=outs, in_specs=[anywhere] * 10, out_specs...  3.35 us

profile of v3, /device:TPU:0, one launch (start us, length us, event | category | flops | bytes accessed | tf_op | source)
XLA Modules:
  0.0 95.7 jit_solution(8606286312844581542)
XLA Ops:
  0.6 91.7 %exchange.1 = (f32[256,640]{1,0:T(8,128)S(1)}, f32[256,640]{1,0:T(8,128)S(1)}, bf16[2048,640]{1,0:T(8,128)(2,1)S(1)}, f32[32,640]{1,0:T(8,128)S(1)}, f32[32,640]...) custom-call(bf16[2048,2048]{1,0:T(8,128)(2,1)} %h_hbm.1, ...), custom_call_target="tpu_custom_call" | custom-call | tf_op jit(solution)/shard_map/exchange/pallas_call | solution.py:600
  92.4 3.4 %flush.1 = (f32[256,640]{1,0:T(8,128)}, f32[256,640]{1,0:T(8,128)}, bf16[2048,640]{1,0:T(8,128)(2,1)}, f32[32,640]{1,0:T(8,128)}, f32[32,640]{1,0:T(8,128)}, /*i...) custom-call(f32[256,640]{1,0:T(8,128)S(1)} %get-tuple-element.20.ref, ...), custom_call_target="tpu_custom_call" | custom-call | tf_op jit(solution)/shard_map/flush/pallas_call | solution.py:653
